TPU v7x, 32 devices: a whole 2x2x4 slice. The times are simulated.
32 devices in a mesh: sp: 8 (over z, core), tp: 4 (over y, x).
Axes of the slice: x: 2, y: 2, z: 4, core: 2. Of those that a mesh axis runs over, the one named last changes fastest.
Arguments:
- tokens: bfloat16 [2048, 4096], P('sp'), may hold values from -6 to 6
- norm_gain: float32 [2, 4096], replicated, may hold values from 0.1 to 1.9
- w_outer: bfloat16 [2, 4096, 1024], P(None, 'sp', 'tp'), may hold values from -0.09375 to 0.09375
- w_inner: bfloat16 [2, 4096, 1024], P(None, 'sp', 'tp'), may hold values from -0.09375 to 0.09375
- w_value: bfloat16 [2, 4096, 1024], P(None, 'sp', 'tp'), may hold values from -0.09375 to 0.09375
- w_back: bfloat16 [2, 1024, 4096], P(None, 'sp', 'tp'), may hold values from -0.1875 to 0.1875
- taps: float32 [2, 3, 1024], P(None, None, 'tp'), may hold values from -3 to 3
Outputs:
- result: bfloat16 [2048, 4096], P('sp', 'tp')
All inputs are finite; a program needn't handle non-finite values.
Results may differ from a plain program's by a relative error of at most 0.022.
Values may be sent and summed in bfloat16 or wider, within the bound.
A program may use at most 64 MiB of HBM per device.

v0:
```python
import jax
import jax.numpy as jnp
from jax import lax
from jax.sharding import PartitionSpec as P

eps = 1e-06


def shifted(block, axis, distance):
    devices = range(lax.axis_size(axis))
    route = [(i - distance, i) for i in devices if i - distance in devices]
    return lax.ppermute(block, axis, route)


def per_device(tokens, norm_gain, w_outer, w_inner, w_value, w_back, taps):
    layers = w_outer.shape[0]
    count = tokens.shape[0]
    feats = w_back.shape[2]
    own = lax.axis_index("tp")
    held = (
        lax.all_gather(w_outer, "sp", axis=1, tiled=True),
        lax.all_gather(w_inner, "sp", axis=1, tiled=True),
        lax.all_gather(w_value, "sp", axis=1, tiled=True),
        lax.all_gather(w_back, "sp", axis=1, tiled=True),
    )
    current = tokens
    resid = lax.dynamic_slice_in_dim(tokens, own * feats, feats, 1)
    for layer in range(layers):
        if layer > 0:
            current = lax.all_gather(resid, "tp", axis=1, tiled=True)
        xf = current.astype(jnp.float32)
        normed = (
            xf * lax.rsqrt(jnp.mean(xf * xf, axis=-1, keepdims=True) + eps) * norm_gain[layer]
        ).astype(jnp.bfloat16)
        outer = jnp.dot(normed, held[0][layer], preferred_element_type=jnp.float32)
        inner = jnp.dot(normed, held[1][layer], preferred_element_type=jnp.float32)
        value = jnp.dot(normed, held[2][layer], preferred_element_type=jnp.float32)
        outer = outer.astype(jnp.bfloat16)
        inner = inner.astype(jnp.bfloat16)
        value = value.astype(jnp.bfloat16)
        mixed = (inner.astype(jnp.float32) * value.astype(jnp.float32)).astype(jnp.bfloat16)
        before = shifted(mixed[count - 2 :], "sp", 1)
        padded = jnp.concatenate([before, mixed], axis=0).astype(jnp.float32)
        conv = (
            taps[layer, 0] * padded[:count]
            + taps[layer, 1] * padded[1 : count + 1]
            + taps[layer, 2] * padded[2:]
        )
        gated = (outer.astype(jnp.float32) * conv).astype(jnp.bfloat16)
        whole = lax.all_gather(gated, "tp", axis=1, tiled=True)
        proj = jnp.dot(whole, held[3][layer], preferred_element_type=jnp.float32)
        resid = (resid.astype(jnp.float32) + proj).astype(jnp.bfloat16)
    return resid


def solution(mesh):
    in_specs = (
        P("sp", None),
        P(),
        P(None, "sp", "tp"),
        P(None, "sp", "tp"),
        P(None, "sp", "tp"),
        P(None, "sp", "tp"),
        P(None, None, "tp"),
    )
    out_specs = P("sp", "tp")
    return jax.shard_map(
        per_device, mesh=mesh, in_specs=in_specs, out_specs=out_specs, check_vma=False
    )
```

profile of v0, /device:TPU:0, one launch (start us, length us, event | category | flops | bytes accessed | tf_op | source)
XLA Modules:
  0.0 271.6 jit_solution(8346042315905669766)
XLA Ops:
  6.5 0.0 copy-start
  6.5 0.0 copy-start.3
  6.5 0.0 all-gather.10.cloned.1.call-start
  6.5 0.7 all-gather.10.cloned.1.call-update
  7.3 0.0 all-gather.8.cloned.1.call-start
  7.3 0.7 all-gather.8.cloned.1.call-update
  8.0 0.0 all-gather.6.cloned.1.call-start
  8.1 0.7 all-gather.6.cloned.1.call-update
  8.7 0.0 all-gather.12.cloned.1.call-start
  8.8 0.5 all-gather.12.cloned.1.call-update
  9.3 0.0 all-gather.14.cloned.1.call-start
  9.4 2.1 fusion
  11.5 0.0 copy-done.3
  11.5 47.1 %all-gather.10.cloned.1.call-done = bf16[2,4096,256]{2,1,0:T(8,128)(2,1)} async-done(((bf16[2,512,256]{2,1,0:T(8,128)(2,1)}), bf16[2,4096,256]{2,1,0:T(8,128)(2,1)}) %all-gather.10.cloned.1.call-update) | async-done | bytes 4194320 | tf_op jit(solution)/shard_map/all_gather | solution.py:23
  58.6 0.0 copy-done
  58.6 2.4 fusion.27
  60.9 0.0 copy-start.4
  60.9 44.9 %all-gather.8.cloned.1.call-done = bf16[2,4096,256]{2,1,0:T(8,128)(2,1)} async-done(((bf16[2,512,256]{2,1,0:T(8,128)(2,1)}), bf16[2,4096,256]{2,1,0:T(8,128)(2,1)}) %all-gather.8.cloned.1.call-update) | async-done | bytes 4194320 | tf_op jit(solution)/shard_map/all_gather | solution.py:22
  105.9 2.4 fusion.25
  108.3 2.1 collective-permute-start
  110.4 0.0 copy-done.4
  110.4 0.8 collective-permute-done
  111.2 42.0 %all-gather.6.cloned.1.call-done = bf16[2,4096,256]{2,1,0:T(8,128)(2,1)} async-done(((bf16[2,512,256]{2,1,0:T(8,128)(2,1)}), bf16[2,4096,256]{2,1,0:T(8,128)(2,1)}) %all-gather.6.cloned.1.call-update) | async-done | bytes 4194320 | tf_op jit(solution)/shard_map/all_gather | solution.py:21
  153.2 2.4 fusion.21
  155.6 14.2 %all_gather.24 = bf16[256,1024]{1,0:T(8,128)(2,1)S(1)} all-gather(bf16[256,256]{1,0:T(8,128)(2,1)S(1)} %fusion.21), channel_id=1, replica_groups=mesh['sp'=8,'tp'=4] {'tp'}, dimensions={1}, use_global_device_ids=true | all-gather | bytes 655360 | tf_op jit(solution)/shard_map/all_gather | solution.py:50
  169.8 30.6 %all-gather.12.cloned.1.call-done = bf16[2,1024,1024]{2,1,0:T(8,128)(2,1)} async-done(((bf16[2,128,1024]{2,1,0:T(8,128)(2,1)}), bf16[2,1024,1024]{2,1,0:T(8,128)(2,1)}) %all-gather.12.cloned.1.call-update) | async-done | bytes 4194320 | tf_op jit(solution)/shard_map/all_gather | solution.py:24
  200.4 3.1 %fusion.17 = bf16[256,1024]{1,0:T(8,128)(2,1)} fusion(bf16[256,1024]{1,0:T(8,128)(2,1)S(1)} %all_gather.24, bf16[2,1024,1024]{2,1,0:T(8,128)(2,1)} %all-gather.12.cloned.1.call-done, bf16[256,4096]{1,0:T(8,128)(2,1)S(1)} %copy-done, s32[]{:T(128)S(6)} %select_n.3), kind=kOutput, calls=%fused_computation.29 | convolution fusion | flops 537657344 | bytes 3670020 | tf_op jit(solution)/shard_map/dot_general | solution.py:51
  203.5 0.0 all-gather.14.cloned.1.call-update
  203.5 34.1 %all-gather.14.cloned.1.call-done = bf16[256,4096]{1,0:T(8,128)(2,1)} async-done(((bf16[256,1024]{1,0:T(8,128)(2,1)}), bf16[256,4096]{1,0:T(8,128)(2,1)}) %all-gather.14.cloned.1.call-update) | async-done | bytes 2097168 | tf_op jit(solution)/shard_map/all_gather | solution.py:30
  237.6 2.1 fusion.3
  239.7 0.0 copy-start.1
  239.7 0.0 copy-start.7
  239.7 3.1 %fusion.37 = f32[256,256]{1,0:T(8,128)S(1)} fusion(bf16[2,4096,256]{2,1,0:T(8,128)(2,1)} %all-gather.10.cloned.1.call-done, bf16[256,4096]{1,0:T(8,128)(2,1)} %all-gather.14.cloned.1.call-done, f32[4096]{0:T(1024)S(1)} %bitcast.82, f32[256]{0:T(256)S(1)} %add_rsqrt_fusion), kind=kOutput, calls=%fused_computation.49 | convolution fusion | flops 541196288 | bytes 4473856 | tf_op jit(solution)/shard_map/dot_general | solution.py:37
  242.9 0.0 copy-done.1
  242.9 0.9 copy-done.7
  243.8 0.0 copy-start.6
  243.8 0.8 fusion.35
  244.6 1.7 collective-permute-start.1
  246.3 0.8 collective-permute-done.1
  247.2 0.0 copy-done.6
  247.2 0.0 copy-start.2
  247.2 0.0 copy-start.5
  247.2 0.8 fusion.31
  248.0 15.6 %all_gather.27 = bf16[256,1024]{1,0:T(8,128)(2,1)S(1)} all-gather(bf16[256,256]{1,0:T(8,128)(2,1)S(1)} %fusion.31), channel_id=1, replica_groups=mesh['sp'=8,'tp'=4] {'tp'}, dimensions={1}, use_global_device_ids=true | all-gather | bytes 655360 | tf_op jit(solution)/shard_map/all_gather | solution.py:50
  263.6 0.0 copy-done.2
  263.6 0.0 copy-done.5
  263.6 1.5 fusion.16
  (8 shorter events, 0.1 us)
Async XLA Ops:
  6.5 52.0 %copy-start = (bf16[256,4096]{1,0:T(8,128)(2,1)S(1)}, bf16[256,4096]{1,0:T(8,128)(2,1)}, u32[]{:S(2)}) copy-start(bf16[256,4096]{1,0:T(8,128)(2,1)} %param.7) | copy-start | bytes 6291460
  6.5 4.9 %copy-start.3 = (f32[2,4096]{1,0:T(2,128)S(1)}, f32[2,4096]{1,0:T(2,128)}, u32[]{:S(2)}) copy-start(f32[2,4096]{1,0:T(2,128)} %param.8) | copy-start | bytes 98308
  6.5 52.0 %all-gather.10.cloned.1.call-start = ((), (), s32[]{:S(2)}) async-start(), calls=%async_computation.2 | async-start | bytes 4718592 | tf_op jit(solution)/shard_map/all_gather | solution.py:23
  7.3 98.6 %all-gather.8.cloned.1.call-start = ((), (), s32[]{:S(2)}) async-start(), calls=%async_computation.1 | async-start | bytes 4718592 | tf_op jit(solution)/shard_map/all_gather | solution.py:22
  8.0 145.2 %all-gather.6.cloned.1.call-start = ((), (), s32[]{:S(2)}) async-start(), calls=%async_computation | async-start | bytes 4718592 | tf_op jit(solution)/shard_map/all_gather | solution.py:21
  8.7 191.6 %all-gather.12.cloned.1.call-start = ((), (), s32[]{:S(2)}) async-start(), calls=%async_computation.3 | async-start | bytes 4718592 | tf_op jit(solution)/shard_map/all_gather | solution.py:24
  9.3 228.3 %all-gather.14.cloned.1.call-start = ((), (), s32[]{:S(2)}) async-start(), calls=%async_computation.4 | async-start | bytes 2621440 | tf_op jit(solution)/shard_map/all_gather | solution.py:30
  60.9 49.5 %copy-start.4 = (f32[2,3,256]{2,0,1:T(2,128)S(1)}, f32[2,3,256]{2,0,1:T(2,128)}, u32[]{:S(2)}) copy-start(f32[2,3,256]{2,0,1:T(2,128)} %param.13) | copy-start | bytes 18436
  108.3 2.9 %collective-permute-start = (bf16[2,256]{1,0:T(2,128)(2,1)S(1)}, bf16[2,256]{1,0:T(2,128)(2,1)S(1)}, u32[]{:S(2)}, u32[]{:S(2)}) collective-permute-start(bf16[2,256]{1,0:T(2,128)(2,1)S(1)} %slice.99), channel_id=1, source_target_pairs={{0,4},{4,8},{8,12},{12,16},{16,20},{20,24},{24,28},{1,5},{5,9},{9,... | collective-permute-start | bytes 3080 | tf_op jit(solution)/shard_map/ppermute | solution.py:12
  239.7 3.2 %copy-start.1 = (bf16[256,4096]{1,0:T(8,128)(2,1)S(1)}, bf16[256,4096]{1,0:T(8,128)(2,1)}, u32[]{:S(2)}) copy-start(bf16[256,4096]{1,0:T(8,128)(2,1)} %all-gather.14.cloned.1.call-done) | copy-start | bytes 6291460
  239.7 4.1 %copy-start.7 = (bf16[2,4096,256]{2,1,0:T(8,128)(2,1)S(1)}, bf16[2,4096,256]{2,1,0:T(8,128)(2,1)}, u32[]{:S(2)}) copy-start(bf16[2,4096,256]{2,1,0:T(8,128)(2,1)} %all-gather.8.cloned.1.call-done) | copy-start | bytes 12582916
  243.8 3.4 %copy-start.6 = (bf16[2,4096,256]{2,1,0:T(8,128)(2,1)S(1)}, bf16[2,4096,256]{2,1,0:T(8,128)(2,1)}, u32[]{:S(2)}) copy-start(bf16[2,4096,256]{2,1,0:T(8,128)(2,1)} %all-gather.6.cloned.1.call-done) | copy-start | bytes 12582916
  244.6 2.5 collective-permute-start.1
  247.2 16.4 %copy-start.2 = (bf16[256,1024]{1,0:T(8,128)(2,1)S(1)}, bf16[256,1024]{1,0:T(8,128)(2,1)}, u32[]{:S(2)}) copy-start(bf16[256,1024]{1,0:T(8,128)(2,1)} %fusion.17) | copy-start | bytes 1572868
  247.2 16.4 %copy-start.5 = (bf16[2,1024,1024]{2,1,0:T(8,128)(2,1)S(1)}, bf16[2,1024,1024]{2,1,0:T(8,128)(2,1)}, u32[]{:S(2)}) copy-start(bf16[2,1024,1024]{2,1,0:T(8,128)(2,1)} %all-gather.12.cloned.1.call-done) | copy-start | bytes 12582916
Sparse Core Ops, SparseCore 0:
  8.9 49.5 all-gather.9
  60.2 45.6 all-gather.7
  107.5 45.6 all-gather.5
  154.7 45.6 all-gather.11
  203.6 33.9 all-gather.13
where the time goes:
time: 272 us
  waiting for transfers between devices  203 us (75%)
  blocking collectives  29.8 us (11%)
  matrix products  16.4 us (6%)
  between operations  13.3 us (5%)
  other arithmetic  4.24 us (2%)
  starting transfers between devices  4 us (1%)
    all_gather x1, waiting for transfers between devices, per_device(): lax.all_gather(w_value, 'sp', axis=1, tiled=True)  47.1 us
    all_gather x1, waiting for transfers between devices, per_device(): lax.all_gather(w_inner, 'sp', axis=1, tiled=True)  44.9 us
    all_gather x1, waiting for transfers between devices, per_device(): lax.all_gather(w_outer, 'sp', axis=1, tiled=True)  42 us
    all_gather x1, waiting for transfers between devices, per_device(): current = lax.all_gather(resid, 'tp', axis=1, tiled=True)  34.1 us
    all_gather x1, waiting for transfers between devices, per_device(): lax.all_gather(w_back, 'sp', axis=1, tiled=True)  30.6 us
    all_gather x2, blocking collectives, per_device(): whole = lax.all_gather(gated, 'tp', axis=1, tiled=True)  29.8 us
    dot_general x2, matrix products, per_device(): value = jnp.dot(normed, held[2][layer], preferred_element_type=jnp.float32)  5.48 us
  transfers between devices with their start and end apart: 7, of which 7 were waited for; matrix products, arithmetic and copies ran while one was open for 3% of the time, Pallas kernels for 0%

commit v1 on v0

--- a/solution.py
+++ b/solution.py
@@ -4,6 +4,12 @@
 from jax.sharding import PartitionSpec as P
 
 eps = 1e-06
+
+
+def gather_blocks(x, axis, dim):
+    parts = lax.all_gather(x, axis, axis=0, tiled=False)
+    whole = jnp.concatenate(parts, axis=dim)
+    return whole
 
 
 def shifted(block, axis, distance):
@@ -19,7 +25,7 @@
     own = lax.axis_index("tp")
     held = (
         lax.all_gather(w_outer, "sp", axis=1, tiled=True),
-        lax.all_gather(w_inner, "sp", axis=1, tiled=True),
+        gather_blocks(w_inner, "sp", 1),
         lax.all_gather(w_value, "sp", axis=1, tiled=True),
         lax.all_gather(w_back, "sp", axis=1, tiled=True),
     )

time: 272 us -> 271 us (level)
  local copies, waits for them, and re-layouts: 0.99 us -> 4.15 us
  waiting for transfers between devices: 203 us -> 200 us
    all_gather x1, waiting for transfers between devices: 47.1 us -> 42.4 us  [per_device(): lax.all_gather(w_value, 'sp', axis=1, tiled=True)]
    slice x0 -> x1, local copies, waits for them, and re-layouts: none -> 4.07 us  [per_device(): inner = jnp.dot(normed, held[1][layer], preferred_element_type=jnp.float32)]
  transfers between devices with their start and end apart: 7 -> 7, of which waited for: 7 -> 7; matrix products, arithmetic and copies ran while one was open for 3% -> 4% of each run, Pallas kernels for 0% -> 0%
where the time goes in v1:
time: 271 us
  waiting for transfers between devices  200 us (74%)
  blocking collectives  29.8 us (11%)
  matrix products  15 us (6%)
  between operations  13.3 us (5%)
  other arithmetic  4.4 us (2%)
  local copies, waits for them, and re-layouts  4.15 us (2%)
  starting transfers between devices  3.98 us (1%)
    all_gather x1, waiting for transfers between devices, gather_blocks(): parts = lax.all_gather(x, axis, axis=0, tiled=False)  47.1 us
    all_gather x1, waiting for transfers between devices, per_device(): lax.all_gather(w_value, 'sp', axis=1, tiled=True)  42.4 us
    all_gather x1, waiting for transfers between devices, per_device(): lax.all_gather(w_outer, 'sp', axis=1, tiled=True)  41.9 us
    all_gather x1, waiting for transfers between devices, per_device(): current = lax.all_gather(resid, 'tp', axis=1, tiled=True)  34.1 us
    all_gather x1, waiting for transfers between devices, per_device(): lax.all_gather(w_back, 'sp', axis=1, tiled=True)  30.5 us
    all_gather x2, blocking collectives, per_device(): whole = lax.all_gather(gated, 'tp', axis=1, tiled=True)  29.8 us
  transfers between devices with their start and end apart: 7, of which 7 were waited for; matrix products, arithmetic and copies ran while one was open for 4% of the time, Pallas kernels for 0%

profile of v1, /device:TPU:0, one launch (start us, length us, event | category | flops | bytes accessed | tf_op | source)
XLA Modules:
  0.0 270.9 jit_solution(9452329579553354569)
XLA Ops:
  6.5 0.0 copy-start.3
  6.5 0.0 all-gather.15.cloned.1.call-start
  6.5 0.7 all-gather.15.cloned.1.call-update
  7.3 0.0 all-gather.9.cloned.1.call-start
  7.3 0.7 all-gather.9.cloned.1.call-update
  8.0 0.0 all-gather.7.cloned.1.call-start
  8.1 0.7 all-gather.7.cloned.1.call-update
  8.7 0.0 all-gather.11.cloned.1.call-start
  8.8 0.5 all-gather.11.cloned.1.call-update
  9.3 0.0 all-gather.13.cloned.1.call-start
  9.4 2.1 fusion
  11.5 0.0 copy-done.3
  11.5 47.1 %all-gather.15.cloned.1.call-done = bf16[16,512,256]{2,1,0:T(8,128)(2,1)} async-done(((bf16[2,512,256]{2,1,0:T(8,128)(2,1)}), bf16[16,512,256]{2,1,0:T(8,128)(2,1)}) %all-gather.15.cloned.1.call-update) | async-done | bytes 4194320 | tf_op jit(solution)/shard_map/all_gather | solution.py:10
  58.6 0.0 copy-start
  58.6 4.1 %fusion.44 = (bf16[1,8,512,256]{3,2,0,1:T(8,128)(2,1)S(1)}, bf16[1,8,512,256]{3,2,0,1:T(8,128)(2,1)}) fusion(bf16[2,8,512,256]{3,2,0,1:T(8,128)(2,1)} %bitcast.75), kind=kLoop, calls=%fused_computation.60 | loop fusion | bytes 8388608 | tf_op jit(solution)/shard_map/slice | solution.py:42
  62.6 0.0 copy-done
  62.6 0.8 fusion.33
  63.4 0.0 copy-start.4
  63.5 42.4 %all-gather.9.cloned.1.call-done = bf16[2,4096,256]{2,1,0:T(8,128)(2,1)} async-done(((bf16[2,512,256]{2,1,0:T(8,128)(2,1)}), bf16[2,4096,256]{2,1,0:T(8,128)(2,1)}) %all-gather.9.cloned.1.call-update) | async-done | bytes 4194320 | tf_op jit(solution)/shard_map/all_gather | solution.py:29
  105.9 2.4 fusion.23
  108.3 2.1 collective-permute-start
  110.4 0.0 copy-done.4
  110.4 0.8 collective-permute-done
  111.2 41.9 %all-gather.7.cloned.1.call-done = bf16[2,4096,256]{2,1,0:T(8,128)(2,1)} async-done(((bf16[2,512,256]{2,1,0:T(8,128)(2,1)}), bf16[2,4096,256]{2,1,0:T(8,128)(2,1)}) %all-gather.7.cloned.1.call-update) | async-done | bytes 4194320 | tf_op jit(solution)/shard_map/all_gather | solution.py:27
  153.2 2.4 fusion.19
  155.6 14.2 %all_gather.28 = bf16[256,1024]{1,0:T(8,128)(2,1)S(1)} all-gather(bf16[256,256]{1,0:T(8,128)(2,1)S(1)} %fusion.19), channel_id=1, replica_groups=mesh['sp'=8,'tp'=4] {'tp'}, dimensions={1}, use_global_device_ids=true | all-gather | bytes 655360 | tf_op jit(solution)/shard_map/all_gather | solution.py:56
  169.8 30.5 %all-gather.11.cloned.1.call-done = bf16[2,1024,1024]{2,1,0:T(8,128)(2,1)} async-done(((bf16[2,128,1024]{2,1,0:T(8,128)(2,1)}), bf16[2,1024,1024]{2,1,0:T(8,128)(2,1)}) %all-gather.11.cloned.1.call-update) | async-done | bytes 4194320 | tf_op jit(solution)/shard_map/all_gather | solution.py:30
  200.3 3.1 %fusion.15 = bf16[256,1024]{1,0:T(8,128)(2,1)} fusion(bf16[256,1024]{1,0:T(8,128)(2,1)S(1)} %all_gather.28, bf16[2,1024,1024]{2,1,0:T(8,128)(2,1)} %all-gather.11.cloned.1.call-done, bf16[256,4096]{1,0:T(8,128)(2,1)S(1)} %copy-done, s32[]{:T(128)S(6)} %select_n.3), kind=kOutput, calls=%fused_computation.25 | convolution fusion | flops 537657344 | bytes 3670020 | tf_op jit(solution)/shard_map/dot_general | solution.py:57
  203.5 0.0 all-gather.13.cloned.1.call-update
  203.5 34.1 %all-gather.13.cloned.1.call-done = bf16[256,4096]{1,0:T(8,128)(2,1)} async-done(((bf16[256,1024]{1,0:T(8,128)(2,1)}), bf16[256,4096]{1,0:T(8,128)(2,1)}) %all-gather.13.cloned.1.call-update) | async-done | bytes 2097168 | tf_op jit(solution)/shard_map/all_gather | solution.py:36
  237.6 0.0 copy-start.1
  237.6 0.0 copy-start.7
  237.6 2.2 fusion.3
  239.9 3.2 %fusion.32 = f32[256,256]{1,0:T(8,128)S(1)} fusion(bf16[4096,256]{1,0:T(8,128)(2,1)} %bitcast.76, bf16[256,4096]{1,0:T(8,128)(2,1)} %all-gather.13.cloned.1.call-done, f32[4096]{0:T(1024)S(1)} %bitcast.78, f32[256]{0:T(256)S(1)} %add_rsqrt_fusion), kind=kOutput, calls=%fused_computation.43 | convolution fusion | flops 541196288 | bytes 4473856 | tf_op jit(solution)/shard_map/dot_general | solution.py:42
  243.1 0.0 copy-done.1
  243.1 0.0 copy-done.7
  243.1 0.0 copy-start.6
  243.1 0.8 fusion.31
  243.9 1.7 collective-permute-start.1
  245.6 0.8 collective-permute-done.1
  246.5 0.0 copy-done.6
  246.5 0.0 copy-start.2
  246.5 0.0 copy-start.5
  246.5 0.8 fusion.27
  247.3 15.6 %all_gather.31 = bf16[256,1024]{1,0:T(8,128)(2,1)S(1)} all-gather(bf16[256,256]{1,0:T(8,128)(2,1)S(1)} %fusion.27), channel_id=1, replica_groups=mesh['sp'=8,'tp'=4] {'tp'}, dimensions={1}, use_global_device_ids=true | all-gather | bytes 655360 | tf_op jit(solution)/shard_map/all_gather | solution.py:56
  262.9 0.0 copy-done.2
  262.9 0.0 copy-done.5
  262.9 1.5 fusion.14
  (8 shorter events, 0.1 us)
Async XLA Ops:
  6.5 4.9 %copy-start.3 = (f32[2,4096]{1,0:T(2,128)S(1)}, f32[2,4096]{1,0:T(2,128)}, u32[]{:S(2)}) copy-start(f32[2,4096]{1,0:T(2,128)} %param.8) | copy-start | bytes 98308
  6.5 52.0 %all-gather.15.cloned.1.call-start = ((), (), s32[]{:S(2)}) async-start(), calls=%async_computation.4 | async-start | bytes 4718592 | tf_op jit(solution)/shard_map/all_gather | solution.py:10
  7.3 98.6 %all-gather.9.cloned.1.call-start = ((), (), s32[]{:S(2)}) async-start(), calls=%async_computation.1 | async-start | bytes 4718592 | tf_op jit(solution)/shard_map/all_gather | solution.py:29
  8.0 145.2 %all-gather.7.cloned.1.call-start = ((), (), s32[]{:S(2)}) async-start(), calls=%async_computation | async-start | bytes 4718592 | tf_op jit(solution)/shard_map/all_gather | solution.py:27
  8.7 191.6 %all-gather.11.cloned.1.call-start = ((), (), s32[]{:S(2)}) async-start(), calls=%async_computation.2 | async-start | bytes 4718592 | tf_op jit(solution)/shard_map/all_gather | solution.py:30
  9.3 228.3 %all-gather.13.cloned.1.call-start = ((), (), s32[]{:S(2)}) async-start(), calls=%async_computation.3 | async-start | bytes 2621440 | tf_op jit(solution)/shard_map/all_gather | solution.py:36
  58.6 4.1 %copy-start = (bf16[256,4096]{1,0:T(8,128)(2,1)S(1)}, bf16[256,4096]{1,0:T(8,128)(2,1)}, u32[]{:S(2)}) copy-start(bf16[256,4096]{1,0:T(8,128)(2,1)} %param.7) | copy-start | bytes 6291460
  63.4 47.0 %copy-start.4 = (f32[2,3,256]{2,0,1:T(2,128)S(1)}, f32[2,3,256]{2,0,1:T(2,128)}, u32[]{:S(2)}) copy-start(f32[2,3,256]{2,0,1:T(2,128)} %param.13) | copy-start | bytes 18436
  108.3 2.9 %collective-permute-start = (bf16[2,256]{1,0:T(2,128)(2,1)S(1)}, bf16[2,256]{1,0:T(2,128)(2,1)S(1)}, u32[]{:S(2)}, u32[]{:S(2)}) collective-permute-start(bf16[2,256]{1,0:T(2,128)(2,1)S(1)} %slice.101), channel_id=1, source_target_pairs={{0,4},{4,8},{8,12},{12,16},{16,20},{20,24},{24,28},{1,5},{5,9},{9,... | collective-permute-start | bytes 3080 | tf_op jit(solution)/shard_map/ppermute | solution.py:18
  237.6 5.5 %copy-start.1 = (bf16[256,4096]{1,0:T(8,128)(2,1)S(1)}, bf16[256,4096]{1,0:T(8,128)(2,1)}, u32[]{:S(2)}) copy-start(bf16[256,4096]{1,0:T(8,128)(2,1)} %all-gather.13.cloned.1.call-done) | copy-start | bytes 6291460
  237.6 5.5 %copy-start.7 = (bf16[2,4096,256]{2,1,0:T(8,128)(2,1)S(1)}, bf16[2,4096,256]{2,1,0:T(8,128)(2,1)}, u32[]{:S(2)}) copy-start(bf16[2,4096,256]{2,1,0:T(8,128)(2,1)} %all-gather.9.cloned.1.call-done) | copy-start | bytes 12582916
  243.1 3.4 %copy-start.6 = (bf16[2,4096,256]{2,1,0:T(8,128)(2,1)S(1)}, bf16[2,4096,256]{2,1,0:T(8,128)(2,1)}, u32[]{:S(2)}) copy-start(bf16[2,4096,256]{2,1,0:T(8,128)(2,1)} %all-gather.7.cloned.1.call-done) | copy-start | bytes 12582916
  243.9 2.5 collective-permute-start.1
  246.5 16.4 %copy-start.2 = (bf16[256,1024]{1,0:T(8,128)(2,1)S(1)}, bf16[256,1024]{1,0:T(8,128)(2,1)}, u32[]{:S(2)}) copy-start(bf16[256,1024]{1,0:T(8,128)(2,1)} %fusion.15) | copy-start | bytes 1572868
  246.5 16.4 %copy-start.5 = (bf16[2,1024,1024]{2,1,0:T(8,128)(2,1)S(1)}, bf16[2,1024,1024]{2,1,0:T(8,128)(2,1)}, u32[]{:S(2)}) copy-start(bf16[2,1024,1024]{2,1,0:T(8,128)(2,1)} %all-gather.11.cloned.1.call-done) | copy-start | bytes 12582916
Sparse Core Ops, SparseCore 0:
  8.9 49.5 all-gather.14
  60.2 45.6 all-gather.8
  107.5 45.6 all-gather.6
  154.6 45.6 all-gather.10
  203.6 33.9 all-gather.12
